TPU v7x, 512 devices: a whole 4x8x8 slice. The times are simulated.
512 devices in a mesh: sp: 32 (over z, x), tp: 16 (over y, core).
Axes of the slice: x: 4, y: 8, z: 8, core: 2. Of those that a mesh axis runs over, the one named last changes fastest.
Arguments:
- queries: bfloat16 [12288, 1024], P('sp', 'tp'), may hold values from -6 to 6
- keys: bfloat16 [12288, 1024], P('sp', 'tp'), may hold values from -6 to 6
- values: bfloat16 [12288, 1024], P('sp', 'tp'), may hold values from -6 to 6
- log_cum: float32 [16, 12288], P('tp'), as said below
- residual: bfloat16 [12288, 2048], P('sp', 'tp'), may hold values from -6 to 6
- out_gain: float32 [1024], replicated, may hold values from 0.1 to 1.9
- w_out: bfloat16 [1024, 2048], P(None, 'tp'), may hold values from -0.1875 to 0.1875
- ffn_gain: float32 [2048], replicated, may hold values from 0.1 to 1.9
- routes: int32 [12288, 2], P('sp'), may hold values from 0 to 63, all different within a row; in each aligned block of 384 rows (0 to 383, 384 to 767, ...) at most 24 rows name the same one
- route_weight: float32 [12288, 2], P('sp'), may hold values from 0.25 to 2
- sh_gate: bfloat16 [2048, 512], P(None, 'tp'), may hold values from -0.125 to 0.125
- sh_up: bfloat16 [2048, 512], P(None, 'tp'), may hold values from -0.125 to 0.125
- sh_down: bfloat16 [512, 2048], P(None, 'tp'), may hold values from -0.25 to 0.25
- exp_gate: bfloat16 [64, 2048, 512], P('sp', None, 'tp'), may hold values from -0.125 to 0.125
- exp_up: bfloat16 [64, 2048, 512], P('sp', None, 'tp'), may hold values from -0.125 to 0.125
- exp_down: bfloat16 [64, 512, 2048], P('sp', None, 'tp'), may hold values from -0.25 to 0.25
Outputs:
- result: bfloat16 [12288, 2048], P('sp', 'tp')
Inputs may be any that keep to these rules, and one draw needn't show every extreme that they name: `routes`: in each aligned block of 384 rows no expert is named by more than 24 rows, a bound that some block reaches. `log_cum`: never rises along positions.
All inputs are finite; a program needn't handle non-finite values.
Results may differ from a plain program's by a relative error of at most 0.0095.
Values may be sent and summed in bfloat16 or wider, within the bound.
No kernel may reach another device: no remote copies, remote signals or barrier semaphores. Data moves between devices by JAX's collectives and lax.ppermute only.
A program may use at most 64 MiB of HBM per device.

v0:
```python
import jax
import jax.numpy as jnp
from jax import lax
from jax.sharding import PartitionSpec as P

EPS = 1e-06


def side_by_side(arrays, axis, dim, along):
    ends, at = ([], 0)
    for a in arrays[:-1]:
        at += a.shape[along]
        ends.append(at)
    both = jnp.concatenate(arrays, axis=along)
    return tuple(jnp.split(lax.all_gather(both, axis, axis=dim, tiled=True), ends, axis=along))


def copy_for_each(value, axis):
    copies = jnp.broadcast_to(value, (lax.axis_size(axis), *value.shape))
    return lax.all_to_all(copies, axis, split_axis=0, concat_axis=0, tiled=True)


def joined_along(pieces, dim):
    shape = list(pieces.shape[1:])
    shape[dim] *= pieces.shape[0]
    return jnp.moveaxis(pieces, 0, dim).reshape(shape)


def collect(value, axis, dim):
    pieces = copy_for_each(value, axis)
    return joined_along(pieces, dim)


def rms_scaled(matrix, gain):
    floats = matrix.astype(jnp.float32)
    inverse = lax.rsqrt(jnp.mean(floats * floats, axis=-1, keepdims=True) + EPS)
    return (floats * inverse * gain).astype(jnp.bfloat16)


def gated_hidden(gate, upward):
    return (jax.nn.silu(gate) * upward).astype(jnp.bfloat16)


def per_device(
    queries,
    keys,
    values,
    log_cum,
    residual,
    out_gain,
    w_out,
    ffn_gain,
    routes,
    route_weight,
    sh_gate,
    sh_up,
    sh_down,
    exp_gate,
    exp_up,
    exp_down,
):
    row_count = queries.shape[0]
    heads_here = log_cum.shape[0]
    head_size = queries.shape[1] // heads_here
    scale = head_size ** (-0.5)
    offset = lax.axis_index("sp") * row_count
    query_heads = queries.reshape(row_count, heads_here, head_size)
    query_pos = offset + lax.iota(jnp.int32, row_count)
    cum_query = lax.dynamic_slice_in_dim(log_cum, offset, row_count, 1)
    best = jnp.full((heads_here, row_count), -1e30, jnp.float32)
    key_piece, value_piece = side_by_side((keys, values), "sp", 0, 1)
    count = key_piece.shape[0]
    key_heads = key_piece.reshape(count, heads_here, head_size)
    value_heads = value_piece.reshape(count, heads_here, head_size)
    causal = lax.iota(jnp.int32, count)[None, :] <= query_pos[:, None]
    score = (
        jnp.einsum("qhd,khd->hqk", query_heads, key_heads, preferred_element_type=jnp.float32)
        * scale
    )
    score = jnp.where(causal[None], score + cum_query[:, :, None] - log_cum[:, None, :], -1e30)
    new_best = jnp.maximum(best, jnp.max(score, axis=2))
    weight = jnp.where(causal[None], jnp.exp(score - new_best[:, :, None]), 0.0)
    running_sum = jnp.sum(weight, axis=2)
    weighted = jnp.einsum(
        "hqk,khd->hqd", weight.astype(jnp.bfloat16), value_heads, preferred_element_type=jnp.float32
    )
    best, running_sum, weighted = (new_best, running_sum, weighted)
    head_out = (
        jnp.transpose(weighted / running_sum[:, :, None], (1, 0, 2))
        .reshape(row_count, heads_here * head_size)
        .astype(jnp.bfloat16)
    )
    all_heads = lax.all_gather(head_out, "tp", axis=1, tiled=True)
    mixed = rms_scaled(all_heads, out_gain)
    attended = jnp.dot(mixed, w_out, preferred_element_type=jnp.float32)
    updated = (residual.astype(jnp.float32) + attended).astype(jnp.bfloat16)
    full_rows = collect(updated, "tp", 1)
    normed = rms_scaled(full_rows, ffn_gain)
    width = normed.shape[1]
    shared_part = gated_hidden(
        jnp.dot(normed, sh_gate, preferred_element_type=jnp.float32),
        jnp.dot(normed, sh_up, preferred_element_type=jnp.float32),
    )
    shared_all = lax.all_gather(shared_part, "tp", axis=1, tiled=True)
    shared_out = jnp.dot(shared_all, sh_down, preferred_element_type=jnp.float32)
    top_count = routes.shape[1]
    expert_local = exp_gate.shape[0]
    sp_count = lax.axis_size("sp")
    tp_count = lax.axis_size("tp")
    expert_count = expert_local * sp_count
    capacity = 2 * row_count * top_count // expert_count
    assigned = routes.reshape(-1)
    onehot = (assigned[:, None] == lax.iota(jnp.int32, expert_count)[None, :]).astype(jnp.int32)
    slot_rank = jnp.sum((jnp.cumsum(onehot, axis=0) - 1) * onehot, axis=1)
    slot = assigned * capacity + slot_rank
    owner_row = lax.iota(jnp.int32, assigned.shape[0]) // top_count
    table = jnp.full((expert_count * capacity,), row_count, jnp.int32).at[slot].set(owner_row)
    padded = jnp.concatenate([normed, jnp.zeros((1, width), jnp.bfloat16)], axis=0)
    outgoing = padded[table].reshape(sp_count, expert_local * capacity, width)
    share = expert_local * capacity // tp_count
    portion = lax.dynamic_slice_in_dim(outgoing, lax.axis_index("tp") * share, share, 1)
    landed = lax.all_to_all(portion, "sp", split_axis=0, concat_axis=0, tiled=True)
    arrived = lax.all_gather(landed, "tp", axis=1, tiled=True)
    arrived = arrived.reshape(sp_count, expert_local, capacity, width)
    gate_part = jnp.einsum("secd,edf->secf", arrived, exp_gate, preferred_element_type=jnp.float32)
    up_part = jnp.einsum("secd,edf->secf", arrived, exp_up, preferred_element_type=jnp.float32)
    hidden = gated_hidden(gate_part, up_part)
    hidden_all = lax.all_gather(hidden, "tp", axis=3, tiled=True)
    expert_out = jnp.einsum(
        "secf,efd->secd", hidden_all, exp_down, preferred_element_type=jnp.float32
    ).astype(jnp.bfloat16)
    returned = lax.all_to_all(expert_out, "sp", split_axis=0, concat_axis=0, tiled=True)
    returned = returned.reshape(expert_count * capacity, returned.shape[3])
    picked = returned[slot].astype(jnp.float32) * route_weight.reshape(-1)[:, None]
    routed = jnp.sum(picked.reshape(row_count, top_count, picked.shape[1]), axis=1)
    return (updated.astype(jnp.float32) + shared_out + routed).astype(jnp.bfloat16)


def solution(mesh):
    in_specs = (
        P("sp", "tp"),
        P("sp", "tp"),
        P("sp", "tp"),
        P("tp", None),
        P("sp", "tp"),
        P(),
        P(None, "tp"),
        P(),
        P("sp", None),
        P("sp", None),
        P(None, "tp"),
        P(None, "tp"),
        P(None, "tp"),
        P("sp", None, "tp"),
        P("sp", None, "tp"),
        P("sp", None, "tp"),
    )
    out_specs = P("sp", "tp")
    return jax.shard_map(
        per_device, mesh=mesh, in_specs=in_specs, out_specs=out_specs, check_vma=False
    )
```

profile of v0, /device:TPU:1, one launch (start us, length us, event | category | flops | bytes accessed | tf_op | source)
XLA Modules:
  0.0 371.9 jit_solution(12435414797633586448)
XLA Ops:
  6.5 1.5 pad_maximum_fusion
  8.8 88.6 %all-gather.4.cloned.1.call-done = bf16[12288,128]{0,1:T(8,128)(2,1)} async-done(((bf16[384,128]{0,1:T(8,128)(2,1)}), bf16[12288,128]{0,1:T(8,128)(2,1)}) %all-gather.4.cloned.1.call-update) | async-done | bytes 3145744 | tf_op jit(solution)/shard_map/all_gather | solution.py:15
  97.4 8.4 %fusion.60 = (f32[384]{0:T(512)S(1)}, f32[384,12288]{0,1:T(8,128)S(1)}) fusion(f32[12288]{0:T(1024)} %bitcast.74, f32[384]{0:T(512)S(1)} %dynamic-slice_reduce_fusion, bf16[384,64]{0,1:T(8,128)(2,1)} %param.16, bf16[12288,128]{0,1:T(8,128)(2,1)} %all-gather.4.cloned.1.call-done, s32[384]{0:T(512)S(1)} %iota_add_fusion), kind=kOutput, calls=%fused_computation.79 | convolution fusion | flops 632290944 | bytes 20550144 | tf_op jit(solution)/shard_map/qhd,khd->hqk/dot_general | solution.py:77
  105.9 4.8 %fusion = f32[384]{0:T(512)S(1)} fusion(f32[384,12288]{0,1:T(8,128)S(1)} %get-tuple-element.6, f32[384]{0:T(512)S(1)} %broadcast_maximum_fusion, s32[384]{0:T(512)S(1)} %iota_add_fusion), kind=kLoop, calls=%fused_computation.6 | loop fusion | flops 18873984 | bytes 18878976 | tf_op jit(solution)/shard_map/reduce_sum | solution.py:83
  110.6 3.7 %fusion.38 = bf16[384,64]{0,1:T(8,128)(2,1)S(1)} fusion(f32[384,12288]{0,1:T(8,128)S(1)} %get-tuple-element.6, f32[384]{0:T(512)S(1)} %broadcast_maximum_fusion, s32[384]{0:T(512)S(1)} %iota_add_fusion, bf16[12288,128]{0,1:T(8,128)(2,1)S(1)} %copy-done.6, f32[384]{0:T(512)S(1)} %fusion), kind=kOutput, calls=%fused_computation.40 | convolution fusion | flops 622903296 | bytes 20502528 | tf_op jit(solution)/shard_map/hqk,khd->hqd/dot_general | solution.py:84
  114.4 23.0 %all_gather.16 = bf16[384,1024]{0,1:T(8,128)(2,1)S(1)} all-gather(bf16[384,64]{0,1:T(8,128)(2,1)S(1)} %fusion.38), channel_id=1, replica_groups=mesh['sp'=32,'tp'=16] {'tp'}, dimensions={1}, use_global_device_ids=true | all-gather | bytes 835584 | tf_op jit(solution)/shard_map/all_gather | solution.py:93
  138.3 1.5 broadcast_in_dim.18
  139.8 4.7 %all-to-all-start = ((bf16[16,384,128]{2,1,0:T(8,128)(2,1)}), bf16[16,384,128]{2,1,0:T(8,128)(2,1)S(1)}, u32[]{:S(2)}, u32[]{:S(2)}) async-start(bf16[16,384,128]{2,1,0:T(8,128)(2,1)} %broadcast_in_dim.18), calls=%async_computation | async-start | bytes 3145728 | tf_op jit(solution)/shard_map/all_to_all | solution.py:20
  145.0 1.8 reduce-window.6
  147.6 3.4 scatter_custom_fusion
  151.0 32.0 %all-to-all-done = bf16[16,384,128]{2,1,0:T(8,128)(2,1)S(1)} async-done(((bf16[16,384,128]{2,1,0:T(8,128)(2,1)}), bf16[16,384,128]{2,1,0:T(8,128)(2,1)S(1)}, u32[]{:S(2)}, u32[]{:S(2)}) %all-to-all-start) | async-done | bytes 1572896 | tf_op jit(solution)/shard_map/all_to_all | solution.py:20
  184.0 7.1 %gather_fusion = bf16[1536,2048]{1,0:T(8,128)(2,1)} fusion(bf16[385,2048]{1,0:T(8,128)(2,1)S(1)} %concatenate.7, s32[2048]{0:T(1024)S(1)} %pad_clamp_fusion), kind=kCustom, calls=%fused_computation | custom fusion | bytes 12589056 | tf_op jit(solution)/shard_map/gather | solution.py:119
  191.1 2.0 constant_dynamic-slice_fusion
  193.1 24.7 %all_to_all.15 = bf16[32,3,2048]{2,1,0:T(4,128)(2,1)S(1)} all-to-all(bf16[32,3,2048]{2,1,0:T(4,128)(2,1)S(1)} %constant_dynamic-slice_fusion), channel_id=1, replica_groups=mesh['sp'=32,'tp'=16] {'sp'}, dimensions={0} | all-to-all | bytes 786432 | tf_op jit(solution)/shard_map/all_to_all | solution.py:122
  218.9 42.5 %all-gather.6.cloned.1.call-done = bf16[32,48,2048]{2,0,1:T(8,128)(2,1)} async-done(((bf16[32,3,2048]{2,0,1:T(8,128)(2,1)}), bf16[32,48,2048]{2,0,1:T(8,128)(2,1)}) %all-gather.6.cloned.1.call-update) | async-done | bytes 6291472 | tf_op jit(solution)/shard_map/all_gather | solution.py:123
  261.4 7.5 %fusion.16 = f32[32,2,24,32]{3,2,0,1:T(8,128)S(1)} fusion(bf16[32,2,24,2048]{3,0,2,1:T(8,128)(2,1)} %bitcast.75, bf16[2,2048,32]{1,2,0:T(8,128)(2,1)} %param.29), kind=kOutput, calls=%fused_computation.26 | convolution fusion | flops 201326592 | bytes 6750208 | tf_op jit(solution)/shard_map/secd,edf->secf/dot_general | solution.py:125
  269.0 4.7 %fusion.25 = bf16[32,2,24,32]{3,2,0,1:T(8,128)(2,1)S(1)} fusion(bf16[32,2,24,2048]{3,0,2,1:T(8,128)(2,1)S(1)} %bitcast.76, f32[32,2,24,32]{3,2,0,1:T(8,128)S(1)} %fusion.16, bf16[2,2048,32]{1,2,0:T(8,128)(2,1)S(1)} %copy-done.8), kind=kOutput, calls=%fused_computation.30 | convolution fusion | flops 201621504 | bytes 6848512 | tf_op jit(solution)/shard_map/secd,edf->secf/dot_general | solution.py:126
  274.9 47.6 %all-gather.8.cloned.1.call-done = bf16[32,2,24,512]{0,2,1,3:T(8,128)(2,1)} async-done(((bf16[32,2,24,32]{0,2,1,3:T(8,128)(2,1)}), bf16[32,2,24,512]{0,2,1,3:T(8,128)(2,1)}) %all-gather.8.cloned.1.call-update) | async-done | bytes 1572880 | tf_op jit(solution)/shard_map/all_gather | solution.py:128
  322.5 7.4 %copy.48 = bf16[32,2,24,512]{3,2,0,1:T(8,128)(2,1)S(1)} copy(bf16[32,2,24,512]{0,2,1,3:T(8,128)(2,1)} %all-gather.8.cloned.1.call-done) | data formatting | bytes 3145728 | tf_op jit(solution)/shard_map/all_gather | solution.py:128
  331.3 9.9 %all-to-all-start.2 = ((bf16[32,2,24,128]{3,2,1,0:T(8,128)(2,1)}), bf16[32,2,24,128]{3,2,1,0:T(8,128)(2,1)S(1)}, u32[]{:S(2)}, u32[]{:S(2)}) async-start(bf16[32,2,24,128]{3,2,1,0:T(8,128)(2,1)} %copy.49), calls=%async_computation.2 | async-start | bytes 786432 | tf_op jit(solution)/shard_map/all_to_all | solution.py:132
  341.4 1.5 fusion.61
  342.9 1.5 fusion.32
  344.4 17.5 %all_gather.17 = bf16[384,512]{0,1:T(8,128)(2,1)S(1)} all-gather(bf16[384,32]{0,1:T(8,128)(2,1)S(1)} %fusion.32), channel_id=1, replica_groups=mesh['sp'=32,'tp'=16] {'tp'}, dimensions={1}, use_global_device_ids=true | all-gather | bytes 417792 | tf_op jit(solution)/shard_map/all_gather | solution.py:104
  361.9 1.9 gather_fusion.1
  (61 shorter events, 9.3 us)
Async XLA Ops:
  6.5 323.4 %copy-start = (bf16[2,512,128]{2,1,0:T(8,128)(2,1)S(1)}, bf16[2,512,128]{2,1,0:T(8,128)(2,1)}, u32[]{:S(2)}) copy-start(bf16[2,512,128]{2,1,0:T(8,128)(2,1)} %param.31) | copy-start | bytes 786436
  6.5 90.9 %all-gather.4.cloned.1.call-start = ((), (), s32[]{:S(2)}) async-start(), calls=%async_computation.3 | async-start | bytes 3244032 | tf_op jit(solution)/shard_map/all_gather | solution.py:15
  105.8 4.8 %copy-start.6 = (bf16[12288,128]{0,1:T(8,128)(2,1)S(1)}, bf16[12288,128]{0,1:T(8,128)(2,1)}, u32[]{:S(2)}) copy-start(bf16[12288,128]{0,1:T(8,128)(2,1)} %all-gather.4.cloned.1.call-done) | copy-start | bytes 9437188
  110.6 27.1 %copy-start.7 = (bf16[1024,128]{1,0:T(8,128)(2,1)S(1)}, bf16[1024,128]{1,0:T(8,128)(2,1)}, u32[]{:S(2)}) copy-start(bf16[1024,128]{1,0:T(8,128)(2,1)} %param.22) | copy-start | bytes 786436
  110.6 27.0 %copy-start.9 = (bf16[384,128]{1,0:T(8,128)(2,1)S(1)}, bf16[384,128]{1,0:T(8,128)(2,1)}, u32[]{:S(2)}) copy-start(bf16[384,128]{1,0:T(8,128)(2,1)} %param.20) | copy-start | bytes 294916
  110.6 27.0 %copy-start.10 = (f32[1024]{0:T(1024)S(1)}, f32[1024]{0:T(1024)}, u32[]{:S(2)}) copy-start(f32[1024]{0:T(1024)} %param.21) | copy-start | bytes 12292
  114.4 30.1 %copy-start.2 = (s32[384,2]{0,1:T(2,128)S(1)}, s32[384,2]{0,1:T(2,128)}, u32[]{:S(2)}) copy-start(s32[384,2]{0,1:T(2,128)} %param.24) | copy-start | bytes 9220
  137.7 45.7 %copy-start.3 = (f32[2048]{0:T(1024)S(1)}, f32[2048]{0:T(1024)}, u32[]{:S(2)}) copy-start(f32[2048]{0:T(1024)} %param.23) | copy-start | bytes 24580
  139.8 43.2 %all-to-all-start = ((bf16[16,384,128]{2,1,0:T(8,128)(2,1)}), bf16[16,384,128]{2,1,0:T(8,128)(2,1)S(1)}, u32[]{:S(2)}, u32[]{:S(2)}) async-start(bf16[16,384,128]{2,1,0:T(8,128)(2,1)} %broadcast_in_dim.18), calls=%async_computation | async-start | bytes 3145728 | tf_op jit(solution)/shard_map/all_to_all | solution.py:20
  144.5 116.9 %all-gather.6.cloned.1.call-start = ((), (), s32[]{:S(2)}) async-start(), calls=%async_computation.4 | async-start | bytes 6684672 | tf_op jit(solution)/shard_map/all_gather | solution.py:123
  218.8 103.6 %all-gather.8.cloned.1.call-start = ((), (), s32[]{:S(2)}) async-start(), calls=%async_computation.5 | async-start | bytes 6684672 | tf_op jit(solution)/shard_map/all_gather | solution.py:128
  261.4 7.5 %copy-start.5 = (bf16[32,48,2048]{2,0,1:T(8,128)(2,1)S(1)}, bf16[32,48,2048]{2,0,1:T(8,128)(2,1)}, u32[]{:S(2)}) copy-start(bf16[32,48,2048]{2,0,1:T(8,128)(2,1)} %all-gather.6.cloned.1.call-done) | copy-start | bytes 18874372
  261.4 7.5 %copy-start.8 = (bf16[2,2048,32]{1,2,0:T(8,128)(2,1)S(1)}, bf16[2,2048,32]{1,2,0:T(8,128)(2,1)}, u32[]{:S(2)}) copy-start(bf16[2,2048,32]{1,2,0:T(8,128)(2,1)} %param.30) | copy-start | bytes 786436
  274.9 66.4 %copy-start.4 = (f32[384,2]{0,1:T(2,128)S(1)}, f32[384,2]{0,1:T(2,128)}, u32[]{:S(2)}) copy-start(f32[384,2]{0,1:T(2,128)} %param.25) | copy-start | bytes 9220
  330.5 33.8 %copy-start.1 = (bf16[512,128]{1,0:T(8,128)(2,1)S(1)}, bf16[512,128]{1,0:T(8,128)(2,1)}, u32[]{:S(2)}) copy-start(bf16[512,128]{1,0:T(8,128)(2,1)} %param.28) | copy-start | bytes 393220
  331.3 30.6 %all-to-all-start.2 = ((bf16[32,2,24,128]{3,2,1,0:T(8,128)(2,1)}), bf16[32,2,24,128]{3,2,1,0:T(8,128)(2,1)S(1)}, u32[]{:S(2)}, u32[]{:S(2)}) async-start(bf16[32,2,24,128]{3,2,1,0:T(8,128)(2,1)} %copy.49), calls=%async_computation.2 | async-start | bytes 786432 | tf_op jit(solution)/shard_map/all_to_all | solution.py:132
Sparse Core Ops, SparseCore 0:
  10.4 86.9 all-gather.3
  219.0 42.3 all-gather.5
  275.0 47.4 all-gather.7
where the time goes:
time: 372 us
  waiting for transfers between devices  211 us (57%)
  blocking collectives  65.2 us (18%)
  matrix products  29.4 us (8%)
  local copies, waits for them, and re-layouts  28.4 us (8%)
  starting transfers between devices  14.6 us (4%)
  between operations  13.5 us (4%)
  other arithmetic  9.93 us (3%)
    all_gather x1, waiting for transfers between devices, side_by_side(): lax.all_gather(both, axis, axis=dim, tiled=True)  88.6 us
    all_gather x1, waiting for transfers between devices, per_device(): hidden_all = lax.all_gather(hidden, 'tp', axis=3, tiled=True)  47.6 us
    all_gather x1, waiting for transfers between devices, per_device(): arrived = lax.all_gather(landed, 'tp', axis=1, tiled=True)  42.5 us
    all_to_all x1, waiting for transfers between devices, copy_for_each(): return lax.all_to_all(copies, axis, split_axis=0, concat_axis=0, tiled=True)  32 us
    all_to_all x1, blocking collectives, per_device(): lax.all_to_all(portion, 'sp', split_axis=0, concat_axis=0, tiled=True)  24.7 us
    all_gather x1, blocking collectives, per_device(): all_heads = lax.all_gather(head_out, 'tp', axis=1, tiled=True)  23 us
    all_gather x1, blocking collectives, per_device(): shared_all = lax.all_gather(shared_part, 'tp', axis=1, tiled=True)  17.5 us
    all_to_all x1, starting transfers between devices, per_device(): lax.all_to_all(expert_out, 'sp', split_axis=0, concat_axis=0, tiled=True)  9.9 us
  transfers between devices with their start and end apart: 5, of which 4 were waited for; matrix products, arithmetic and copies ran while one was open for 3% of the time, Pallas kernels for 0%

commit v1 on v0

--- a/solution.py
+++ b/solution.py
@@ -90,7 +90,12 @@
         .reshape(row_count, heads_here * head_size)
         .astype(jnp.bfloat16)
     )
-    all_heads = lax.all_gather(head_out, "tp", axis=1, tiled=True)
+
+    def ports_tell(array_in):
+        k_now = jnp.concatenate(lax.all_gather(array_in, "tp"), 1)
+        return k_now
+
+    all_heads = ports_tell(head_out)
     mixed = rms_scaled(all_heads, out_gain)
     attended = jnp.dot(mixed, w_out, preferred_element_type=jnp.float32)
     updated = (residual.astype(jnp.float32) + attended).astype(jnp.bfloat16)

time: 372 us -> 373 us (level)
  no operation moved by 1% of the time
where the time goes in v1:
time: 373 us; the launch traced here: 372 us
  waiting for transfers between devices  211 us (57%)
  blocking collectives  65.2 us (17%)
  matrix products  29.2 us (8%)
  local copies, waits for them, and re-layouts  29.1 us (8%)
  starting transfers between devices  14.6 us (4%)
  between operations  13.5 us (4%)
  other arithmetic  10.2 us (3%)
    all_gather x1, waiting for transfers between devices, side_by_side(): lax.all_gather(both, axis, axis=dim, tiled=True)  88.6 us
    all_gather x1, waiting for transfers between devices, per_device(): hidden_all = lax.all_gather(hidden, 'tp', axis=3, tiled=True)  47.6 us
    all_gather x1, waiting for transfers between devices, per_device(): arrived = lax.all_gather(landed, 'tp', axis=1, tiled=True)  42.5 us
    all_to_all x1, waiting for transfers between devices, copy_for_each(): return lax.all_to_all(copies, axis, split_axis=0, concat_axis=0, tiled=True)  31.8 us
    all_to_all x1, blocking collectives, per_device(): lax.all_to_all(portion, 'sp', split_axis=0, concat_axis=0, tiled=True)  24.7 us
    all_gather x1, blocking collectives, ports_tell(): k_now = jnp.concatenate(lax.all_gather(array_in, 'tp'), 1)  23 us
    all_gather x1, blocking collectives, per_device(): shared_all = lax.all_gather(shared_part, 'tp', axis=1, tiled=True)  17.5 us
    all_to_all x1, starting transfers between devices, per_device(): lax.all_to_all(expert_out, 'sp', split_axis=0, concat_axis=0, tiled=True)  9.9 us
  transfers between devices with their start and end apart: 5, of which 4 were waited for; matrix products, arithmetic and copies ran while one was open for 3% of the time, Pallas kernels for 0%

profile of v1, /device:TPU:1, one launch (start us, length us, event | category | flops | bytes accessed | tf_op | source)
XLA Modules:
  0.0 372.4 jit_solution(17976360601174268218)
XLA Ops:
  6.5 1.5 pad_maximum_fusion
  8.8 88.6 %all-gather.5.cloned.1.call-done = bf16[12288,128]{0,1:T(8,128)(2,1)} async-done(((bf16[384,128]{0,1:T(8,128)(2,1)}), bf16[12288,128]{0,1:T(8,128)(2,1)}) %all-gather.5.cloned.1.call-update) | async-done | bytes 3145744 | tf_op jit(solution)/shard_map/all_gather | solution.py:15
  97.4 8.4 %fusion.57 = (f32[384]{0:T(512)S(1)}, f32[384,12288]{0,1:T(8,128)S(1)}) fusion(f32[12288]{0:T(1024)} %bitcast.97, f32[384]{0:T(512)S(1)} %dynamic-slice_reduce_fusion, bf16[384,64]{0,1:T(8,128)(2,1)} %param.16, bf16[12288,128]{0,1:T(8,128)(2,1)} %all-gather.5.cloned.1.call-done, s32[384]{0:T(512)S(1)} %iota_add_fusion), kind=kOutput, calls=%fused_computation.78 | convolution fusion | flops 632290944 | bytes 20550144 | tf_op jit(solution)/shard_map/qhd,khd->hqk/dot_general | solution.py:77
  105.9 4.8 %fusion = f32[384]{0:T(512)S(1)} fusion(f32[384,12288]{0,1:T(8,128)S(1)} %get-tuple-element.6, f32[384]{0:T(512)S(1)} %broadcast_maximum_fusion, s32[384]{0:T(512)S(1)} %iota_add_fusion), kind=kLoop, calls=%fused_computation.6 | loop fusion | flops 18873984 | bytes 18878976 | tf_op jit(solution)/shard_map/reduce_sum | solution.py:83
  110.6 3.7 %fusion.38 = bf16[384,64]{0,1:T(8,128)(2,1)S(1)} fusion(f32[384,12288]{0,1:T(8,128)S(1)} %get-tuple-element.6, f32[384]{0:T(512)S(1)} %broadcast_maximum_fusion, s32[384]{0:T(512)S(1)} %iota_add_fusion, bf16[12288,128]{0,1:T(8,128)(2,1)S(1)} %copy-done.9, f32[384]{0:T(512)S(1)} %fusion), kind=kOutput, calls=%fused_computation.41 | convolution fusion | flops 622903296 | bytes 20502528 | tf_op jit(solution)/shard_map/hqk,khd->hqd/dot_general | solution.py:84
  114.4 23.0 %all-gather = bf16[6144,64]{0,1:T(8,128)(2,1)S(1)} all-gather(bf16[384,64]{0,1:T(8,128)(2,1)S(1)} %fusion.38), channel_id=2, replica_groups=mesh['sp'=32,'tp'=16] {'tp'}, dimensions={0}, use_global_device_ids=true | all-gather | bytes 835584 | tf_op jit(solution)/shard_map/all_gather | solution.py:95
  138.9 1.5 broadcast_in_dim.18
  140.3 4.7 %all-to-all-start = ((bf16[16,384,128]{2,1,0:T(8,128)(2,1)}), bf16[16,384,128]{2,1,0:T(8,128)(2,1)S(1)}, u32[]{:S(2)}, u32[]{:S(2)}) async-start(bf16[16,384,128]{2,1,0:T(8,128)(2,1)} %broadcast_in_dim.18), calls=%async_computation | async-start | bytes 3145728 | tf_op jit(solution)/shard_map/all_to_all | solution.py:20
  145.5 1.8 reduce-window.6
  148.1 3.6 scatter_custom_fusion
  151.7 31.8 %all-to-all-done = bf16[16,384,128]{2,1,0:T(8,128)(2,1)S(1)} async-done(((bf16[16,384,128]{2,1,0:T(8,128)(2,1)}), bf16[16,384,128]{2,1,0:T(8,128)(2,1)S(1)}, u32[]{:S(2)}, u32[]{:S(2)}) %all-to-all-start) | async-done | bytes 1572896 | tf_op jit(solution)/shard_map/all_to_all | solution.py:20
  184.6 7.1 %gather_fusion = bf16[1536,2048]{1,0:T(8,128)(2,1)} fusion(bf16[385,2048]{1,0:T(8,128)(2,1)S(1)} %concatenate.7, s32[2048]{0:T(1024)S(1)} %pad_clamp_fusion), kind=kCustom, calls=%fused_computation | custom fusion | bytes 12589056 | tf_op jit(solution)/shard_map/gather | solution.py:124
  191.7 2.0 constant_dynamic-slice_fusion
  193.6 24.7 %all_to_all.15 = bf16[32,3,2048]{2,1,0:T(4,128)(2,1)S(1)} all-to-all(bf16[32,3,2048]{2,1,0:T(4,128)(2,1)S(1)} %constant_dynamic-slice_fusion), channel_id=1, replica_groups=mesh['sp'=32,'tp'=16] {'sp'}, dimensions={0} | all-to-all | bytes 786432 | tf_op jit(solution)/shard_map/all_to_all | solution.py:127
  219.4 42.5 %all-gather.7.cloned.1.call-done = bf16[32,48,2048]{2,0,1:T(8,128)(2,1)} async-done(((bf16[32,3,2048]{2,0,1:T(8,128)(2,1)}), bf16[32,48,2048]{2,0,1:T(8,128)(2,1)}) %all-gather.7.cloned.1.call-update) | async-done | bytes 6291472 | tf_op jit(solution)/shard_map/all_gather | solution.py:128
  262.0 7.5 %fusion.16 = f32[32,2,24,32]{3,2,0,1:T(8,128)S(1)} fusion(bf16[32,2,24,2048]{3,0,2,1:T(8,128)(2,1)} %bitcast.98, bf16[2,2048,32]{1,2,0:T(8,128)(2,1)} %param.29), kind=kOutput, calls=%fused_computation.27 | convolution fusion | flops 201326592 | bytes 6750208 | tf_op jit(solution)/shard_map/secd,edf->secf/dot_general | solution.py:130
  269.5 4.7 %fusion.25 = bf16[32,2,24,32]{3,2,0,1:T(8,128)(2,1)S(1)} fusion(bf16[32,2,24,2048]{3,0,2,1:T(8,128)(2,1)S(1)} %bitcast.99, f32[32,2,24,32]{3,2,0,1:T(8,128)S(1)} %fusion.16, bf16[2,2048,32]{1,2,0:T(8,128)(2,1)S(1)} %copy-done.10), kind=kOutput, calls=%fused_computation.31 | convolution fusion | flops 201621504 | bytes 6848512 | tf_op jit(solution)/shard_map/secd,edf->secf/dot_general | solution.py:131
  275.4 47.6 %all-gather.9.cloned.1.call-done = bf16[32,2,24,512]{0,2,1,3:T(8,128)(2,1)} async-done(((bf16[32,2,24,32]{0,2,1,3:T(8,128)(2,1)}), bf16[32,2,24,512]{0,2,1,3:T(8,128)(2,1)}) %all-gather.9.cloned.1.call-update) | async-done | bytes 1572880 | tf_op jit(solution)/shard_map/all_gather | solution.py:133
  323.0 7.4 %copy.51 = bf16[32,2,24,512]{3,2,0,1:T(8,128)(2,1)S(1)} copy(bf16[32,2,24,512]{0,2,1,3:T(8,128)(2,1)} %all-gather.9.cloned.1.call-done) | data formatting | bytes 3145728 | tf_op jit(solution)/shard_map/all_gather | solution.py:133
  331.9 9.9 %all-to-all-start.2 = ((bf16[32,2,24,128]{3,2,1,0:T(8,128)(2,1)}), bf16[32,2,24,128]{3,2,1,0:T(8,128)(2,1)S(1)}, u32[]{:S(2)}, u32[]{:S(2)}) async-start(bf16[32,2,24,128]{3,2,1,0:T(8,128)(2,1)} %copy.52), calls=%async_computation.2 | async-start | bytes 786432 | tf_op jit(solution)/shard_map/all_to_all | solution.py:137
  341.9 1.5 fusion.58
  343.4 1.5 fusion.32
  344.9 17.5 %all_gather.18 = bf16[384,512]{0,1:T(8,128)(2,1)S(1)} all-gather(bf16[384,32]{0,1:T(8,128)(2,1)S(1)} %fusion.32), channel_id=1, replica_groups=mesh['sp'=32,'tp'=16] {'tp'}, dimensions={1}, use_global_device_ids=true | all-gather | bytes 417792 | tf_op jit(solution)/shard_map/all_gather | solution.py:109
  362.4 1.9 gather_fusion.1
  (65 shorter events, 9.8 us)
Async XLA Ops:
  6.5 323.9 %copy-start = (bf16[2,512,128]{2,1,0:T(8,128)(2,1)S(1)}, bf16[2,512,128]{2,1,0:T(8,128)(2,1)}, u32[]{:S(2)}) copy-start(bf16[2,512,128]{2,1,0:T(8,128)(2,1)} %param.31) | copy-start | bytes 786436
  6.5 90.9 %all-gather.5.cloned.1.call-start = ((), (), s32[]{:S(2)}) async-start(), calls=%async_computation.3 | async-start | bytes 3244032 | tf_op jit(solution)/shard_map/all_gather | solution.py:15
  105.8 4.8 %copy-start.9 = (bf16[12288,128]{0,1:T(8,128)(2,1)S(1)}, bf16[12288,128]{0,1:T(8,128)(2,1)}, u32[]{:S(2)}) copy-start(bf16[12288,128]{0,1:T(8,128)(2,1)} %all-gather.5.cloned.1.call-done) | copy-start | bytes 9437188
  137.4 0.8 copy-start.6
  137.5 1.0 copy-start.1
  137.5 1.0 copy-start.3
  138.1 6.9 %copy-start.4 = (s32[384,2]{0,1:T(2,128)S(1)}, s32[384,2]{0,1:T(2,128)}, u32[]{:S(2)}) copy-start(s32[384,2]{0,1:T(2,128)} %param.24) | copy-start | bytes 9220
  138.5 45.5 %copy-start.5 = (f32[2048]{0:T(1024)S(1)}, f32[2048]{0:T(1024)}, u32[]{:S(2)}) copy-start(f32[2048]{0:T(1024)} %param.23) | copy-start | bytes 24580
  140.3 43.2 %all-to-all-start = ((bf16[16,384,128]{2,1,0:T(8,128)(2,1)}), bf16[16,384,128]{2,1,0:T(8,128)(2,1)S(1)}, u32[]{:S(2)}, u32[]{:S(2)}) async-start(bf16[16,384,128]{2,1,0:T(8,128)(2,1)} %broadcast_in_dim.18), calls=%async_computation | async-start | bytes 3145728 | tf_op jit(solution)/shard_map/all_to_all | solution.py:20
  145.0 116.9 %all-gather.7.cloned.1.call-start = ((), (), s32[]{:S(2)}) async-start(), calls=%async_computation.4 | async-start | bytes 6684672 | tf_op jit(solution)/shard_map/all_gather | solution.py:128
  219.4 103.6 %all-gather.9.cloned.1.call-start = ((), (), s32[]{:S(2)}) async-start(), calls=%async_computation.5 | async-start | bytes 6684672 | tf_op jit(solution)/shard_map/all_gather | solution.py:133
  261.9 7.5 %copy-start.8 = (bf16[32,48,2048]{2,0,1:T(8,128)(2,1)S(1)}, bf16[32,48,2048]{2,0,1:T(8,128)(2,1)}, u32[]{:S(2)}) copy-start(bf16[32,48,2048]{2,0,1:T(8,128)(2,1)} %all-gather.7.cloned.1.call-done) | copy-start | bytes 18874372
  262.0 7.5 %copy-start.10 = (bf16[2,2048,32]{1,2,0:T(8,128)(2,1)S(1)}, bf16[2,2048,32]{1,2,0:T(8,128)(2,1)}, u32[]{:S(2)}) copy-start(bf16[2,2048,32]{1,2,0:T(8,128)(2,1)} %param.30) | copy-start | bytes 786436
  275.4 66.4 %copy-start.7 = (f32[384,2]{0,1:T(2,128)S(1)}, f32[384,2]{0,1:T(2,128)}, u32[]{:S(2)}) copy-start(f32[384,2]{0,1:T(2,128)} %param.25) | copy-start | bytes 9220
  331.1 33.8 %copy-start.2 = (bf16[512,128]{1,0:T(8,128)(2,1)S(1)}, bf16[512,128]{1,0:T(8,128)(2,1)}, u32[]{:S(2)}) copy-start(bf16[512,128]{1,0:T(8,128)(2,1)} %param.28) | copy-start | bytes 393220
  331.9 30.6 %all-to-all-start.2 = ((bf16[32,2,24,128]{3,2,1,0:T(8,128)(2,1)}), bf16[32,2,24,128]{3,2,1,0:T(8,128)(2,1)S(1)}, u32[]{:S(2)}, u32[]{:S(2)}) async-start(bf16[32,2,24,128]{3,2,1,0:T(8,128)(2,1)} %copy.52), calls=%async_computation.2 | async-start | bytes 786432 | tf_op jit(solution)/shard_map/all_to_all | solution.py:137
Sparse Core Ops, SparseCore 0:
  10.4 86.9 all-gather.4
  219.5 42.3 all-gather.6
  275.5 47.4 all-gather.8
